TPU v7x, 512 devices: a whole 4x8x8 slice. The times are simulated.
512 devices in a mesh: ep: 32 (over z, x), tp: 16 (over y, core).
Axes of the slice: x: 4, y: 8, z: 8, core: 2. Of those that a mesh axis runs over, the one named last changes fastest.
Arguments:
- tokens: bfloat16 [1024, 2048], P(('ep', 'tp')), may hold values from -6 to 6
- cache_keys: bfloat16 [1024, 1024, 256], P(('ep', 'tp')), may hold values from -360 to 360
- cache_values: bfloat16 [1024, 1024, 256], P(('ep', 'tp')), may hold values from -6 to 6
- cache_gates: float32 [1024, 2, 1024], P(('ep', 'tp')), may hold values from -256 to 0, as said below
- lengths: int32 [1024], P(('ep', 'tp')), may hold values from 1 to 1024, 524288 in all
- routes: int32 [1024, 4], P(('ep', 'tp')), may hold values from 0 to 31, all different within a row; in each aligned block of 2 rows (0 to 1, 2 to 3, ...) no two rows name the same one
- route_logits: float32 [1024, 4], P(('ep', 'tp')), may hold values from -6 to 6
- attn_gain: float32 [2048], replicated, may hold values from 0.1 to 1.9
- w_query: bfloat16 [2048, 2048], P(None, 'tp'), may hold values from -0.125 to 0.125
- w_keyval: bfloat16 [2048, 512], P(None, 'tp'), may hold values from -0.125 to 0.125
- w_forget: bfloat16 [2048, 2], replicated, may hold values from -0.125 to 0.125
- forget_bias: float32 [2], replicated, may hold values from -1 to 3
- w_out: bfloat16 [2048, 2048], P(None, 'tp'), may hold values from -0.125 to 0.125
- mix_gain: float32 [2048], replicated, may hold values from 0.1 to 1.9
- ffn_gain: float32 [2048], replicated, may hold values from 0.1 to 1.9
- w_gate: bfloat16 [32, 2048, 2048], P('ep', None, 'tp'), may hold values from -0.125 to 0.125
- w_lin: bfloat16 [32, 2048, 2048], P('ep', None, 'tp'), may hold values from -0.125 to 0.125
- gate_bias: float32 [32, 2048], P('ep', 'tp'), may hold values from -12 to 12
- lin_bias: float32 [32, 2048], P('ep', 'tp'), may hold values from -12 to 12
- w_down: bfloat16 [32, 2048, 2048], P('ep', 'tp'), may hold values from -0.125 to 0.125
- post_gain: float32 [2048], replicated, may hold values from 0.1 to 1.9
Outputs:
- updated: bfloat16 [1024, 2048], P(('ep', 'tp'))
- new_entries: bfloat16 [1024, 512], P(('ep', 'tp'))
Inputs may be any that keep to these rules, and one draw needn't show every extreme that they name: `cache_gates`: along the positions of each sequence and head the values never increase. The lengths of all sequences add up to 524288, and some sequence has exactly 1024. `routes`: each row names 4 different experts; among the rows of one device no expert is named twice; every expert is named by some row.
All inputs are finite; a program needn't handle non-finite values. No bound on the sum of `lengths` on one device may be relied on, other than what follows from the above.
Results may differ from a plain program's by a relative error of at most 0.014.
The roundings to bfloat16 on the way count: a program that leaves them out, or rounds other values in their place, can miss the bound.
Values may be sent and summed in bfloat16 or wider, within the bound.
A program may use at most 64 MiB of HBM per device.

v0:
```python
import jax
import jax.numpy as jnp
from jax import lax
from jax.sharding import PartitionSpec as P

HEADS = 16
KVH = 2
HDIM = 128


NORM_EPS = 1e-06
SWIGLU_ALPHA = 1.702
SWIGLU_LIMIT = 7.0
NEG_LARGE = -1e30


def laid_out(tiles, dim):
    shape = list(tiles.shape[1:])
    shape[dim] *= tiles.shape[0]
    return jnp.moveaxis(tiles, 0, dim).reshape(shape)


def sent_to_all(array, axis):
    copies = jnp.broadcast_to(array, (lax.axis_size(axis), *array.shape))
    return lax.all_to_all(copies, axis, split_axis=0, concat_axis=0, tiled=True)


def gather_directly(array, axis, dim):
    return laid_out(sent_to_all(array, axis), dim)


def rms_scale(values, gain):
    values = values.astype(jnp.float32)
    return values * lax.rsqrt(jnp.mean(values * values, axis=-1, keepdims=True) + NORM_EPS) * gain


def clamped_unit(gate, linear):
    gate = jnp.minimum(gate, SWIGLU_LIMIT)
    linear = jnp.clip(linear, -SWIGLU_LIMIT, SWIGLU_LIMIT)
    return gate * jax.nn.sigmoid(SWIGLU_ALPHA * gate) * (linear + 1.0)


def block_scores(q_four, cache_keys, cache_gates, base, lengths, span, scale):
    seqs = cache_keys.shape[0]
    k_four = cache_keys.reshape(seqs, span, q_four.shape[1], q_four.shape[3])
    scores = (
        jnp.einsum("sgqd,spgd->sgqp", q_four, k_four, preferred_element_type=jnp.float32) * scale
    )
    scores = scores + (base[:, :, None, None] - cache_gates[:, :, None, :])
    place = lax.iota(jnp.int32, span)
    live = place[None, None, None, :] < lengths[:, None, None, None]
    return (jnp.where(live, scores, NEG_LARGE), live)


def per_device(
    tokens,
    cache_keys,
    cache_values,
    cache_gates,
    lengths,
    routes,
    route_logits,
    attn_gain,
    w_query,
    w_keyval,
    w_forget,
    forget_bias,
    w_out,
    mix_gain,
    ffn_gain,
    w_gate,
    w_lin,
    gate_bias,
    lin_bias,
    w_down,
    post_gain,
):
    seqs, width = tokens.shape
    normed = rms_scale(tokens, attn_gain).astype(jnp.bfloat16)
    query_cols = w_query.shape[1]
    pair_cols = w_keyval.shape[1]
    piece = gather_directly(normed, "tp", 0)
    both = jnp.concatenate(
        [
            jnp.dot(piece, w_query, preferred_element_type=jnp.float32),
            jnp.dot(piece, w_keyval, preferred_element_type=jnp.float32),
        ],
        axis=1,
    )
    gathered = both.astype(jnp.bfloat16)
    owned = lax.all_to_all(gathered, "tp", split_axis=0, concat_axis=1, tiled=True)
    groups = lax.axis_size("tp")
    owned = owned.reshape(seqs, groups, query_cols + pair_cols)
    query = owned[:, :, :query_cols].reshape(seqs, groups * query_cols)
    fresh = owned[:, :, query_cols:].reshape(seqs, groups * pair_cols)
    forget = jax.nn.log_sigmoid(
        jnp.dot(normed, w_forget, preferred_element_type=jnp.float32) + forget_bias
    )
    q_four = query.reshape(seqs, KVH, HEADS // KVH, HDIM)
    new_key = fresh[:, : KVH * HDIM].reshape(seqs, KVH, HDIM)
    new_value = fresh[:, KVH * HDIM :].reshape(seqs, KVH, HDIM)
    span_all = cache_keys.shape[1]
    place = lax.iota(jnp.int32, span_all)
    last = jnp.sum(
        jnp.where(place[None, None, :] == lengths[:, None, None] - 1, cache_gates, 0.0), axis=2
    )
    base = last + forget
    scale = HDIM ** (-0.5)
    own = jnp.einsum("sgqd,sgd->sgq", q_four, new_key, preferred_element_type=jnp.float32) * scale
    values_four = cache_values.reshape(seqs, span_all, KVH, HDIM)
    masked, live = block_scores(q_four, cache_keys, cache_gates, base, lengths, span_all, scale)
    top = jnp.maximum(jnp.max(masked, axis=-1), own)
    expo = jnp.where(live, jnp.exp(masked - top[..., None]), 0.0)
    own_expo = jnp.exp(own - top)
    total = jnp.sum(expo, axis=-1) + own_expo
    weights = (expo / total[..., None]).astype(jnp.bfloat16)
    mixed = jnp.einsum("sgqp,spgd->sgqd", weights, values_four, preferred_element_type=jnp.float32)
    own_weight = (own_expo / total).astype(jnp.bfloat16)
    mixed = (
        mixed
        + own_weight.astype(jnp.float32)[..., None] * new_value.astype(jnp.float32)[:, :, None, :]
    )
    mixed = mixed.reshape(seqs, HEADS * HDIM).astype(jnp.bfloat16)
    projected = jnp.dot(
        gather_directly(mixed, "tp", 0), w_out, preferred_element_type=jnp.float32
    ).astype(jnp.bfloat16)
    projected = lax.all_to_all(projected, "tp", split_axis=0, concat_axis=1, tiled=True)
    residual = tokens.astype(jnp.float32) + rms_scale(projected, mix_gain)
    expert_in = rms_scale(residual, ffn_gain).astype(jnp.bfloat16)
    experts = lax.axis_size("ep")
    hit = (routes[:, :, None] == lax.iota(jnp.int32, experts)[None, None, :]).astype(jnp.float32)
    probs = jax.nn.softmax(route_logits, axis=-1)
    combine = jnp.sum(probs[:, :, None] * hit, axis=1)
    chosen = jnp.sum(hit, axis=1).T
    outbound = jnp.dot(
        chosen.astype(jnp.bfloat16), expert_in, preferred_element_type=jnp.float32
    ).astype(jnp.bfloat16)[:, None, :]
    slots = outbound.shape[1]
    arrived = lax.all_to_all(outbound, "ep", split_axis=0, concat_axis=0, tiled=True)
    flat = arrived.reshape(experts * slots, width)
    pooled = lax.all_gather(flat, "tp", axis=0, tiled=True)
    piece = pooled
    gate = jnp.dot(piece, w_gate[0], preferred_element_type=jnp.float32) + gate_bias[0]
    linear = jnp.dot(piece, w_lin[0], preferred_element_type=jnp.float32) + lin_bias[0]
    act = clamped_unit(gate, linear).astype(jnp.bfloat16)
    summed = lax.psum_scatter(
        jnp.dot(act, w_down[0], preferred_element_type=jnp.float32).astype(jnp.bfloat16),
        "tp",
        scatter_dimension=0,
        tiled=True,
    )
    returned = lax.all_to_all(
        summed.reshape(experts, slots, width), "ep", split_axis=0, concat_axis=0, tiled=True
    )
    moe = jnp.einsum("se,ed->sd", combine, returned[:, 0, :].astype(jnp.float32))
    updated = (residual + rms_scale(moe, post_gain)).astype(jnp.bfloat16)
    return (updated, fresh)


def solution(mesh):
    in_specs = (
        P(("ep", "tp"), None),
        P(("ep", "tp"), None, None),
        P(("ep", "tp"), None, None),
        P(("ep", "tp"), None, None),
        P(("ep", "tp")),
        P(("ep", "tp"), None),
        P(("ep", "tp"), None),
        P(),
        P(None, "tp"),
        P(None, "tp"),
        P(),
        P(),
        P(None, "tp"),
        P(),
        P(),
        P("ep", None, "tp"),
        P("ep", None, "tp"),
        P("ep", "tp"),
        P("ep", "tp"),
        P("ep", "tp", None),
        P(),
    )
    out_specs = (P(("ep", "tp"), None), P(("ep", "tp"), None))
    return jax.shard_map(
        per_device, mesh=mesh, in_specs=in_specs, out_specs=out_specs, check_vma=False
    )
```

profile of v0, /device:TPU:1, one launch (start us, length us, event | category | flops | bytes accessed | tf_op | source)
XLA Modules:
  0.0 218.2 jit_solution(12834729480745042205)
XLA Ops:
  7.2 0.0 copy-start
  7.2 0.0 copy-start.12
  7.2 1.0 fusion.67
  8.2 0.8 fusion.69
  9.0 0.7 broadcast_in_dim.37
  9.7 10.1 %all-to-all-start = ((bf16[16,2,2048]{2,1,0:T(2,128)(2,1)}), bf16[16,2,2048]{2,1,0:T(2,128)(2,1)S(1)}, u32[]{:S(2)}, u32[]{:S(2)}) async-start(bf16[16,2,2048]{2,1,0:T(2,128)(2,1)} %broadcast_in_dim.37), calls=%async_computation | async-start | bytes 262144 | tf_op jit(solution)/shard_map/all_to_all | solution.py:25
  19.8 0.7 broadcast_add_fusion
  20.5 0.1 iota_compare_fusion
  20.6 0.8 select_reduce_fusion
  21.4 0.8 fusion.77
  22.2 0.8 broadcast_subtract_fusion
  23.0 6.0 %all-to-all-done = bf16[16,2,2048]{2,1,0:T(2,128)(2,1)S(1)} async-done(((bf16[16,2,2048]{2,1,0:T(2,128)(2,1)}), bf16[16,2,2048]{2,1,0:T(2,128)(2,1)S(1)}, u32[]{:S(2)}, u32[]{:S(2)}) %all-to-all-start) | async-done | bytes 131104 | tf_op jit(solution)/shard_map/all_to_all | solution.py:25
  29.0 1.1 convolution_convert_fusion.3
  30.1 0.0 copy-start.4
  30.1 1.3 convolution_convert_fusion.4
  31.4 0.0 copy-start.2
  31.4 0.6 copy.45
  32.0 3.4 %all-to-all-start.1 = ((bf16[16,2,160]{2,1,0:T(2,128)(2,1)}), bf16[16,2,160]{2,1,0:T(2,128)(2,1)S(1)}, u32[]{:S(2)}, u32[]{:S(2)}) async-start(bf16[16,2,160]{2,1,0:T(2,128)(2,1)} %copy.45), calls=%async_computation.1 | async-start | bytes 32768 | tf_op jit(solution)/shard_map/all_to_all | solution.py:91
  35.4 0.7 iota_compare_fusion.1
  36.1 0.8 reduce_max.19
  36.9 5.4 %all-to-all-done.1 = bf16[16,2,160]{2,1,0:T(2,128)(2,1)S(1)} async-done(((bf16[16,2,160]{2,1,0:T(2,128)(2,1)}), bf16[16,2,160]{2,1,0:T(2,128)(2,1)S(1)}, u32[]{:S(2)}, u32[]{:S(2)}) %all-to-all-start.1) | async-done | bytes 10272 | tf_op jit(solution)/shard_map/all_to_all | solution.py:91
  42.4 0.1 reshape.145
  42.5 0.1 fusion.70
  42.6 0.0 copy-done
  42.6 0.0 copy-start.5
  42.6 0.5 fusion.88
  43.1 0.2 fusion.59
  43.3 0.0 copy-done.12
  43.3 0.0 copy-start.10
  43.3 0.3 fusion.31
  43.7 0.7 broadcast_in_dim.42
  44.4 3.7 %all-to-all-start.2 = ((bf16[16,2,2048]{2,1,0:T(2,128)(2,1)}), bf16[16,2,2048]{2,1,0:T(2,128)(2,1)S(1)}, u32[]{:S(2)}, u32[]{:S(2)}) async-start(bf16[16,2,2048]{2,1,0:T(2,128)(2,1)} %broadcast_in_dim.42), calls=%async_computation.2 | async-start | bytes 262144 | tf_op jit(solution)/shard_map/all_to_all | solution.py:25
  48.1 0.2 fusion.80
  48.3 0.1 fusion.79
  48.3 8.9 %all-to-all-done.2 = bf16[16,2,2048]{2,1,0:T(2,128)(2,1)S(1)} async-done(((bf16[16,2,2048]{2,1,0:T(2,128)(2,1)}), bf16[16,2,2048]{2,1,0:T(2,128)(2,1)S(1)}, u32[]{:S(2)}, u32[]{:S(2)}) %all-to-all-start.2) | async-done | bytes 131104 | tf_op jit(solution)/shard_map/all_to_all | solution.py:25
  57.3 0.1 reshape.148
  57.3 0.8 convolution_convert_fusion.2
  58.1 3.4 %all-to-all-start.3 = ((bf16[16,2,128]{2,1,0:T(2,128)(2,1)}), bf16[16,2,128]{2,1,0:T(2,128)(2,1)S(1)}, u32[]{:S(2)}, u32[]{:S(2)}) async-start(bf16[16,2,128]{2,1,0:T(2,128)(2,1)} %bitcast.6), calls=%async_computation.3 | async-start | bytes 16384 | tf_op jit(solution)/shard_map/all_to_all | solution.py:127
  61.5 0.0 all-gather.3.cloned.1.call-start
  61.6 0.1 convert_reduce_fusion
  61.7 6.4 %all-to-all-done.3 = bf16[16,2,128]{2,1,0:T(2,128)(2,1)S(1)} async-done(((bf16[16,2,128]{2,1,0:T(2,128)(2,1)}), bf16[16,2,128]{2,1,0:T(2,128)(2,1)S(1)}, u32[]{:S(2)}, u32[]{:S(2)}) %all-to-all-start.3) | async-done | bytes 8224 | tf_op jit(solution)/shard_map/all_to_all | solution.py:127
  68.1 0.1 fusion.66
  68.2 0.2 multiply_reduce_fusion.1
  68.4 0.2 fusion
  68.7 0.5 broadcast.126
  69.2 0.7 reduce.2
  69.9 0.1 reshape.160
  69.9 0.0 copy-start.11
  70.0 20.5 %all_to_all.46 = bf16[32,2,1024]{2,1,0:T(2,128)(2,1)S(1)} all-to-all(bf16[32,2,1024]{2,1,0:T(2,128)(2,1)S(1)} %reshape.160), channel_id=1, replica_groups=mesh['ep'=32,'tp'=16] {'ep'}, dimensions={0} | all-to-all | bytes 262144 | tf_op jit(solution)/shard_map/all_to_all | solution.py:139
  90.4 0.1 reshape.161
  90.5 0.7 copy.51
  91.3 0.0 all-gather.3.cloned.1.call-update
  91.3 0.0 reduce-scatter.2.cloned.1.call-start
  91.3 33.5 %all-gather.3.cloned.1.call-done = bf16[512,1,2048]{2,0,1:T(8,128)(2,1)} async-done(((bf16[32,1,2048]{2,0,1:T(8,128)(2,1)}), bf16[512,1,2048]{2,0,1:T(8,128)(2,1)}) %all-gather.3.cloned.1.call-update) | async-done | bytes 2097168 | tf_op jit(solution)/shard_map/all_gather | solution.py:141
  124.8 2.5 %fusion.8 = f32[512,128]{1,0:T(8,128)S(1)} fusion(bf16[512,1,2048]{2,0,1:T(8,128)(2,1)} %all-gather.3.cloned.1.call-done, bf16[1,2048,128]{2,1,0:T(8,128)(2,1)} %param.36, f32[128]{0:T(128)S(1)} %bitcast.104), kind=kOutput, calls=%fused_computation.8 | convolution fusion | flops 268566528 | bytes 2884096 | tf_op jit(solution)/shard_map/dot_general | solution.py:143
  127.4 3.8 %convolution_convert_fusion = bf16[512,2048]{1,0:T(8,128)(2,1)} fusion(bf16[512,1,2048]{2,0,1:T(8,128)(2,1)S(1)} %copy-done.1, bf16[1,128,2048]{2,1,0:T(8,128)(2,1)} %param.40, bf16[1,2048,128]{2,1,0:T(8,128)(2,1)} %param.37, f32[512,128]{1,0:T(8,128)S(1)} %fusion.8, f32[128]{0:T(128)S(1)} %bitcast.105), kind=kOutput, calls=%fused_computation | convolution fusion | flops 538574848 | bytes 5505536 | tf_op jit(solution)/shard_map/dot_general | solution.py:147
  131.2 0.0 reduce-scatter.2.cloned.1.call-update
  131.2 59.5 %reduce-scatter.2.cloned.1.call-done = bf16[32,2048]{1,0:T(8,128)(2,1)} async-done(((bf16[512,2048]{1,0:T(8,128)(2,1)}), bf16[32,2048]{1,0:T(8,128)(2,1)}) %reduce-scatter.2.cloned.1.call-update) | async-done | bytes 131088 | tf_op jit(solution)/shard_map/reduce_scatter | solution.py:146
  190.7 1.6 reduce.3
  192.3 0.1 reshape.162
  192.4 17.9 %all_to_all.47 = bf16[32,2,1024]{2,1,0:T(2,128)(2,1)S(1)} all-to-all(bf16[32,2,1024]{2,1,0:T(2,128)(2,1)S(1)} %reshape.162), channel_id=1, replica_groups=mesh['ep'=32,'tp'=16] {'ep'}, dimensions={0} | all-to-all | bytes 262144 | tf_op jit(solution)/shard_map/all_to_all | solution.py:152
  210.2 0.1 reshape.163
  210.3 0.3 multiply_reduce_fusion
  210.7 0.7 add_convert_fusion
  (31 shorter events, 0.2 us)
Async XLA Ops:
  7.2 35.4 %copy-start = (bf16[2,1024,256]{2,1,0:T(8,128)(2,1)S(1)}, bf16[2,1024,256]{2,1,0:T(8,128)(2,1)}, u32[]{:S(2)}) copy-start(bf16[2,1024,256]{2,1,0:T(8,128)(2,1)} %param.22) | copy-start | bytes 3145732
  7.2 36.1 %copy-start.12 = (bf16[2,1024,256]{2,1,0:T(8,128)(2,1)S(1)}, bf16[2,1024,256]{2,1,0:T(8,128)(2,1)}, u32[]{:S(2)}) copy-start(bf16[2,1024,256]{2,1,0:T(8,128)(2,1)} %param.23) | copy-start | bytes 3145732
  9.7 19.3 %all-to-all-start = ((bf16[16,2,2048]{2,1,0:T(2,128)(2,1)}), bf16[16,2,2048]{2,1,0:T(2,128)(2,1)S(1)}, u32[]{:S(2)}, u32[]{:S(2)}) async-start(bf16[16,2,2048]{2,1,0:T(2,128)(2,1)} %broadcast_in_dim.37), calls=%async_computation | async-start | bytes 262144 | tf_op jit(solution)/shard_map/all_to_all | solution.py:25
  30.1 18.0 %copy-start.4 = (f32[2,4]{1,0:T(2,128)S(1)}, f32[2,4]{1,0:T(2,128)}, u32[]{:S(2)}) copy-start(f32[2,4]{1,0:T(2,128)} %param.27) | copy-start | bytes 100
  31.4 25.9 %copy-start.2 = (bf16[2048,128]{1,0:T(8,128)(2,1)S(1)}, bf16[2048,128]{1,0:T(8,128)(2,1)}, u32[]{:S(2)}) copy-start(bf16[2048,128]{1,0:T(8,128)(2,1)} %param.33) | copy-start | bytes 1572868
  32.0 10.3 %all-to-all-start.1 = ((bf16[16,2,160]{2,1,0:T(2,128)(2,1)}), bf16[16,2,160]{2,1,0:T(2,128)(2,1)S(1)}, u32[]{:S(2)}, u32[]{:S(2)}) async-start(bf16[16,2,160]{2,1,0:T(2,128)(2,1)} %copy.45), calls=%async_computation.1 | async-start | bytes 32768 | tf_op jit(solution)/shard_map/all_to_all | solution.py:91
  42.4 15.7 %copy-start.7 = (bf16[2,512]{1,0:T(2,128)(2,1)}, bf16[2,512]{1,0:T(2,128)(2,1)S(1)}, u32[]{:S(2)}) copy-start(bf16[2,512]{1,0:T(2,128)(2,1)S(1)} %reshape.145) | copy-start | bytes 6148
  42.6 19.0 %copy-start.9 = (s32[2,4]{1,0:T(2,128)S(1)}, s32[2,4]{1,0:T(2,128)}, u32[]{:S(2)}) copy-start(s32[2,4]{1,0:T(2,128)} %param.26) | copy-start | bytes 100
  42.6 25.6 %copy-start.3 = (bf16[2,2048]{1,0:T(2,128)(2,1)S(1)}, bf16[2,2048]{1,0:T(2,128)(2,1)}, u32[]{:S(2)}) copy-start(bf16[2,2048]{1,0:T(2,128)(2,1)} %param.21) | copy-start | bytes 24580
  42.6 25.6 %copy-start.8 = (f32[2048]{0:T(1024)S(1)}, f32[2048]{0:T(1024)}, u32[]{:S(2)}) copy-start(f32[2048]{0:T(1024)} %param.34) | copy-start | bytes 24580
  42.6 25.8 %copy-start.5 = (f32[2048]{0:T(1024)S(1)}, f32[2048]{0:T(1024)}, u32[]{:S(2)}) copy-start(f32[2048]{0:T(1024)} %param.35) | copy-start | bytes 24580
  43.3 81.5 %copy-start.10 = (f32[1,128]{1,0:T(1,128)S(1)}, f32[1,128]{1,0:T(1,128)}, u32[]{:S(2)}) copy-start(f32[1,128]{1,0:T(1,128)} %param.38) | copy-start | bytes 1540
  44.4 12.9 %all-to-all-start.2 = ((bf16[16,2,2048]{2,1,0:T(2,128)(2,1)}), bf16[16,2,2048]{2,1,0:T(2,128)(2,1)S(1)}, u32[]{:S(2)}, u32[]{:S(2)}) async-start(bf16[16,2,2048]{2,1,0:T(2,128)(2,1)} %broadcast_in_dim.42), calls=%async_computation.2 | async-start | bytes 262144 | tf_op jit(solution)/shard_map/all_to_all | solution.py:25
  58.1 9.9 %all-to-all-start.3 = ((bf16[16,2,128]{2,1,0:T(2,128)(2,1)}), bf16[16,2,128]{2,1,0:T(2,128)(2,1)S(1)}, u32[]{:S(2)}, u32[]{:S(2)}) async-start(bf16[16,2,128]{2,1,0:T(2,128)(2,1)} %bitcast.6), calls=%async_computation.3 | async-start | bytes 16384 | tf_op jit(solution)/shard_map/all_to_all | solution.py:127
  61.5 63.3 %all-gather.3.cloned.1.call-start = ((), (), s32[]{:S(2)}) async-start(), calls=%async_computation.8 | async-start | bytes 2228224 | tf_op jit(solution)/shard_map/all_gather | solution.py:141
  69.9 57.4 %copy-start.11 = (f32[1,128]{1,0:T(1,128)S(1)}, f32[1,128]{1,0:T(1,128)}, u32[]{:S(2)}) copy-start(f32[1,128]{1,0:T(1,128)} %param.39) | copy-start | bytes 1540
  91.3 99.4 %reduce-scatter.2.cloned.1.call-start = ((), (), s32[]{:S(2)}) async-start(), calls=%async_computation.7 | async-start | bytes 2228224 | tf_op jit(solution)/shard_map/reduce_scatter | solution.py:146
  124.8 2.6 %copy-start.1 = (bf16[512,1,2048]{2,0,1:T(8,128)(2,1)S(1)}, bf16[512,1,2048]{2,0,1:T(8,128)(2,1)}, u32[]{:S(2)}) copy-start(bf16[512,1,2048]{2,0,1:T(8,128)(2,1)} %all-gather.3.cloned.1.call-done) | copy-start | bytes 6291460
  131.2 79.5 %copy-start.6 = (f32[2048]{0:T(1024)S(1)}, f32[2048]{0:T(1024)}, u32[]{:S(2)}) copy-start(f32[2048]{0:T(1024)} %param.41) | copy-start | bytes 24580
Sparse Core Ops, SparseCore 0:
  91.4 33.3 all-gather.2
  131.3 59.3 reduce-scatter.1
where the time goes:
time: 221 us; the launch traced here: 218 us
  waiting for transfers between devices  120 us (54%)
  blocking collectives  38.3 us (17%)
  starting transfers between devices  20.7 us (9%)
  between operations  14.3 us (6%)
  matrix products  11.8 us (5%)
  other arithmetic  9.53 us (4%)
  local copies, waits for them, and re-layouts  3.91 us (2%)
    reduce_scatter x1, waiting for transfers between devices, per_device(): lax.psum_scatter(jnp.dot(act, w_down[0], preferred_element_type=jnp.float...  59.5 us
    all_gather x1, waiting for transfers between devices, per_device(): pooled = lax.all_gather(flat, 'tp', axis=0, tiled=True)  33.5 us
    all_to_all x1, blocking collectives, per_device(): lax.all_to_all(outbound, 'ep', split_axis=0, concat_axis=0, tiled=True)  20.5 us
    all_to_all x1, blocking collectives, per_device(): lax.all_to_all(summed.reshape(experts, slots, width), 'ep', split_axis=0,...  17.9 us
    all_to_all x2, waiting for transfers between devices, sent_to_all(): return lax.all_to_all(copies, axis, split_axis=0, concat_axis=0, tiled=True)  14.9 us
    all_to_all x2, starting transfers between devices, sent_to_all(): return lax.all_to_all(copies, axis, split_axis=0, concat_axis=0, tiled=True)  13.8 us
    all_to_all x1, waiting for transfers between devices, per_device(): lax.all_to_all(projected, 'tp', split_axis=0, concat_axis=1, tiled=True)  6.4 us
    all_to_all x1, waiting for transfers between devices, per_device(): lax.all_to_all(gathered, 'tp', split_axis=0, concat_axis=1, tiled=True)  5.38 us
  transfers between devices with their start and end apart: 6, of which 6 were waited for; matrix products, arithmetic and copies ran while one was open for 2% of the time, Pallas kernels for 0%

commit v1 on v0

--- a/solution.py
+++ b/solution.py
@@ -1,17 +1,24 @@
+import functools
+
 import jax
 import jax.numpy as jnp
 from jax import lax
+from jax.experimental import pallas as pl
+from jax.experimental.pallas import tpu as pltpu
 from jax.sharding import PartitionSpec as P
 
 HEADS = 16
 KVH = 2
 HDIM = 128
-
 
 NORM_EPS = 1e-06
 SWIGLU_ALPHA = 1.702
 SWIGLU_LIMIT = 7.0
 NEG_LARGE = -1e30
+MESH = pl.DeviceIdType.MESH
+CORES = 2
+F32 = jnp.float32
+BF16 = jnp.bfloat16
 
 
 def laid_out(tiles, dim):
@@ -30,7 +37,7 @@
 
 
 def rms_scale(values, gain):
-    values = values.astype(jnp.float32)
+    values = values.astype(F32)
     return values * lax.rsqrt(jnp.mean(values * values, axis=-1, keepdims=True) + NORM_EPS) * gain
 
 
@@ -38,6 +45,301 @@
     gate = jnp.minimum(gate, SWIGLU_LIMIT)
     linear = jnp.clip(linear, -SWIGLU_LIMIT, SWIGLU_LIMIT)
     return gate * jax.nn.sigmoid(SWIGLU_ALPHA * gate) * (linear + 1.0)
+
+
+def goes(way, chunk, reach, half):
+    return 1 <= reach <= (half if way == chunk else half - 1)
+
+
+def remote(src, dst, send_sem, recv_sem, to):
+    return pltpu.make_async_remote_copy(
+        src_ref=src, dst_ref=dst, send_sem=send_sem, recv_sem=recv_sem,
+        device_id=to, device_id_type=MESH,
+    )
+
+
+def arrived(ref, sem):
+    pltpu.make_async_copy(ref, ref, sem).wait()
+
+
+def split_rows(row):
+    half = row.shape[1] // 2
+    return jnp.concatenate([row[:, :half], row[:, half:]], axis=0)
+
+
+def expert_kernel(
+    residual_ref, ffn_gain_ref, post_gain_ref, routes_ref, logits_ref, gate_bias_ref, lin_bias_ref,
+    w_gate_hbm, w_lin_hbm, w_down_hbm,
+    out_ref,
+    w_in, w_down, outbox, inbox, rows, parts, peer_parts, ring_in, ring_out, back_out, back_in,
+    load_sem, go_send, go_recv, self_sem, cw_send, ccw_send, core_send, ring_recv, core_recv,
+    part_send, part_recv, sum_send, sum_recv, back_send, back_recv,
+):
+    eps = lax.axis_size("ep")
+    tps = lax.axis_size("tp")
+    ny = tps // CORES
+    half = ny // 2
+    seqs, width = residual_ref.shape
+    hidden = w_down.shape[0]
+    chunk_rows = eps // 2
+    me_ep = lax.axis_index("ep")
+    me_tp = lax.axis_index("tp")
+    me_y = me_tp // CORES
+    me_c = me_tp % CORES
+
+    def at(shift, core=None):
+        core = me_c if core is None else core
+        return {"tp": lax.rem(me_y + shift + ny, ny) * CORES + core}
+
+    partner = at(0, 1 - me_c)
+
+    loads = [
+        pltpu.make_async_copy(w_gate_hbm.at[0], w_in.at[:, pl.ds(0, hidden)], load_sem.at[0]),
+        pltpu.make_async_copy(w_lin_hbm.at[0], w_in.at[:, pl.ds(hidden, hidden)], load_sem.at[1]),
+        pltpu.make_async_copy(w_down_hbm.at[0], w_down, load_sem.at[2]),
+    ]
+    for load in loads:
+        load.start()
+
+    barrier = pltpu.get_barrier_semaphore()
+    near = [at(1), partner] + ([at(-1)] if ny > 2 else [])
+    for to in near:
+        pl.semaphore_signal(barrier, inc=1, device_id=to, device_id_type=MESH)
+    far_first = sorted(range(1, eps), key=lambda d: -min(d, eps - d))
+    for d in far_first:
+        to = {"ep": lax.rem(me_ep + d, eps)}
+        pl.semaphore_signal(barrier, inc=1, device_id=to, device_id_type=MESH)
+
+    residual = residual_ref[...]
+    expert_in = rms_scale(residual, ffn_gain_ref[...]).astype(BF16).astype(F32)
+    routes = routes_ref[...]
+    top = routes.shape[1]
+    entry = lax.broadcasted_iota(jnp.int32, (2 * eps, 1), 0)
+    owner, side = entry // 2, entry % 2
+    hw = width // 2
+    mail = jnp.zeros((2 * eps, hw), F32)
+    for s in range(seqs):
+        named = functools.reduce(
+            jnp.logical_or, [owner == routes[s : s + 1, k : k + 1] for k in range(top)]
+        )
+        row = expert_in[s : s + 1, :]
+        mail = jnp.where(named & (side == 0), row[:, :hw], mail)
+        mail = jnp.where(named & (side == 1), row[:, hw:], mail)
+    for e in range(eps):
+        outbox[e] = mail[2 * e : 2 * e + 2, :].astype(BF16)
+
+    pl.semaphore_wait(barrier, len(near) + eps - 1)
+    for d in far_first:
+        to = lax.rem(me_ep + d, eps)
+        remote(
+            outbox.at[to], inbox.at[me_ep], go_send, go_recv.at[me_ep // chunk_rows], {"ep": to}
+        ).start()
+    pltpu.make_async_copy(
+        outbox.at[me_ep], inbox.at[me_ep], go_recv.at[me_ep // chunk_rows]
+    ).start()
+
+    probs = jax.nn.softmax(logits_ref[...], axis=-1)
+    lane = lax.broadcasted_iota(jnp.int32, (seqs, eps), 1)
+    combine = jnp.zeros((seqs, eps), F32)
+    for k in range(top):
+        combine += jnp.where(routes[:, k : k + 1] == lane, probs[:, k : k + 1], 0.0)
+
+    def shift_of(slot):
+        if slot == 0:
+            return 0
+        return -slot if slot <= half else slot - half
+
+    def chip(slot):
+        return lax.rem(me_y + shift_of(slot) + ny, ny)
+
+    sends = []
+
+    def pass_on(slot, g):
+        block = rows.at[chip(slot), me_c, g]
+        if slot == 0:
+            ways = [(0, 1), (1, 1)]
+        else:
+            ways = [(0, slot + 1)] if slot <= half else [(1, slot - half + 1)]
+        for way, reach in ways:
+            if goes(way, g, reach, half):
+                there = reach if way == 0 else half + reach
+                sends.append(remote(
+                    block, block, (cw_send if way == 0 else ccw_send).at[slot, g],
+                    ring_recv.at[there, g], at(1 if way == 0 else -1),
+                ))
+                sends[-1].start()
+        sends.append(remote(block, block, core_send.at[slot, g], core_recv.at[slot, g], partner))
+        sends[-1].start()
+
+    for g in range(2):
+        first = g * chunk_rows
+        arrived(inbox.at[pl.ds(first, chunk_rows)], go_recv.at[g])
+        pairs = [inbox[first + i].astype(F32) for i in range(chunk_rows)]
+        rows[me_y, me_c, g] = jnp.concatenate(
+            [
+                jnp.concatenate([pair[0:1] for pair in pairs], axis=0),
+                jnp.concatenate([pair[1:2] for pair in pairs], axis=0),
+            ],
+            axis=1,
+        ).astype(BF16)
+        pass_on(0, g)
+
+    def slots_at(reach):
+        if reach == 0:
+            return [(0, (0, 1))]
+        found = []
+        for way in range(2):
+            gs = tuple(g for g in range(2) if goes(way, g, reach, half))
+            if gs:
+                found.append((reach if way == 0 else half + reach, gs))
+        return found
+
+    def work(reach):
+        slots = slots_at(reach)
+        for slot, gs in slots:
+            for g in gs:
+                block = rows.at[chip(slot), 1 - me_c, g]
+                arrived(block, core_recv.at[slot, g])
+        for slot in [slots[0][0]] if reach == half else [slot for slot, _ in slots]:
+            place = chip(slot)
+            x = rows[place].reshape(4 * chunk_rows, width)
+            both = jnp.dot(x, w_in[...], preferred_element_type=F32)
+            act = clamped_unit(
+                both[:, :hidden] + gate_bias_ref[...], both[:, hidden:] + lin_bias_ref[...]
+            ).astype(BF16)
+            out = jnp.dot(act, w_down[...], preferred_element_type=F32).astype(BF16)
+            parts[place] = out.reshape(2, 2, chunk_rows, width)
+            sends.append(remote(
+                parts.at[place, 1 - me_c], peer_parts.at[place], part_send.at[slot],
+                part_recv.at[slot], partner,
+            ))
+            sends[-1].start()
+
+    for load in loads:
+        load.wait()
+    for reach in range(1, half + 1):
+        for slot, gs in sorted(slots_at(reach), key=lambda pair: pair[1]):
+            for g in gs:
+                arrived(rows.at[chip(slot), me_c, g], ring_recv.at[slot, g])
+                pass_on(slot, g)
+        work(reach - 1)
+    work(half)
+
+    seen = set()
+
+    def local_sum(slot, g):
+        place = chip(slot)
+        if slot not in seen:
+            arrived(peer_parts.at[place], part_recv.at[slot])
+            seen.add(slot)
+        return parts[place, me_c, g].astype(F32) + peer_parts[place, g].astype(F32)
+
+    def inward(way, reach, g):
+        arrived(ring_in.at[way, reach, g], sum_recv.at[way, reach, g])
+        return ring_in[way, reach, g].astype(F32)
+
+    for reach in range(half, 0, -1):
+        for way, g in [(0, 1), (1, 0), (0, 0), (1, 1)]:
+            if not goes(way, g, reach, half):
+                continue
+            slot = half if reach == half else (half + reach if way == 0 else reach)
+            total = local_sum(slot, g)
+            if goes(way, g, reach + 1, half):
+                total += inward(way, reach + 1, g)
+            ring_out[way, reach, g] = total.astype(BF16)
+            sends.append(remote(
+                ring_out.at[way, reach, g], ring_in.at[way, reach, g],
+                sum_send.at[way, reach, g], sum_recv.at[way, reach, g],
+                at(1 if way == 0 else -1),
+            ))
+            sends[-1].start()
+
+    for g in range(2):
+        total = local_sum(0, g)
+        for way in range(2):
+            if goes(way, g, 1, half):
+                total += inward(way, 1, g)
+        for i in range(chunk_rows):
+            back_out[g * chunk_rows + i] = split_rows(total[i : i + 1, :]).astype(BF16)
+        for i in range(chunk_rows):
+            to = g * chunk_rows + i
+
+            @pl.when(me_ep != to)
+            def _():
+                remote(
+                    back_out.at[to], back_in.at[me_ep], back_send, back_recv, {"ep": to}
+                ).start()
+
+            @pl.when(me_ep == to)
+            def _():
+                pltpu.make_async_copy(back_out.at[to], back_in.at[me_ep], back_recv).start()
+
+    arrived(back_in, back_recv)
+    for s in range(seqs):
+        moe = jnp.zeros((2, hw), F32)
+        for e in range(eps):
+            moe += combine[s : s + 1, e : e + 1] * back_in[e].astype(F32)
+        mean = jnp.sum(jnp.sum(moe * moe, axis=1, keepdims=True), axis=0, keepdims=True) / width
+        moe = moe * lax.rsqrt(mean + NORM_EPS) * split_rows(post_gain_ref[...])
+        moe = jnp.concatenate([moe[0:1], moe[1:2]], axis=1)
+        back_sum = residual[s : s + 1, :] + moe
+        out_ref[s : s + 1, :] = back_sum
+
+    for send in sends:
+        send.wait_send()
+    arrived(outbox.at[pl.ds(0, eps - 1)], go_send)
+    arrived(back_out.at[pl.ds(0, eps - 1)], back_send)
+
+
+def run_experts(residual, ffn_gain, post_gain, routes, logits, gate_bias, lin_bias, w_gate, w_lin, w_down):
+    eps = lax.axis_size("ep")
+    ny = lax.axis_size("tp") // CORES
+    half = ny // 2
+    seqs, width = residual.shape
+    hidden = w_down.shape[1]
+    r = eps // 2
+    vmem = pl.BlockSpec(memory_space=pltpu.VMEM)
+    anyspace = pl.BlockSpec(memory_space=pl.ANY)
+    dma = pltpu.SemaphoreType.DMA
+    slots = 2 * half + 1
+    return pl.pallas_call(
+        expert_kernel,
+        out_shape=jax.ShapeDtypeStruct((seqs, width), F32),
+        in_specs=[vmem] * 7 + [anyspace] * 3,
+        out_specs=vmem,
+        scratch_shapes=[
+            pltpu.VMEM((width, 2 * hidden), BF16),
+            pltpu.VMEM((hidden, width), BF16),
+            pltpu.VMEM((eps, 2, width // 2), BF16),
+            pltpu.VMEM((eps, 2, width // 2), BF16),
+            pltpu.VMEM((ny, 2, 2, r, width), BF16),
+            pltpu.VMEM((ny, 2, 2, r, width), BF16),
+            pltpu.VMEM((ny, 2, r, width), BF16),
+            pltpu.VMEM((2, half + 1, 2, r, width), BF16),
+            pltpu.VMEM((2, half + 1, 2, r, width), BF16),
+            pltpu.VMEM((eps, 2, width // 2), BF16),
+            pltpu.VMEM((eps, 2, width // 2), BF16),
+            dma((3,)),
+            dma,
+            dma((2,)),
+            dma,
+            dma((slots, 2)),
+            dma((slots, 2)),
+            dma((slots, 2)),
+            dma((slots, 2)),
+            dma((slots, 2)),
+            dma((slots,)),
+            dma((slots,)),
+            dma((2, half + 1, 2)),
+            dma((2, half + 1, 2)),
+            dma,
+            dma,
+        ],
+        compiler_params=pltpu.CompilerParams(
+            collective_id=0, has_side_effects=True, vmem_limit_bytes=40 * 1024 * 1024
+        ),
+        name="experts",
+    )(residual, ffn_gain, post_gain, routes, logits, gate_bias, lin_bias, w_gate, w_lin, w_down)
 
 
 def block_scores(q_four, cache_keys, cache_gates, base, lengths, span, scale):
@@ -126,35 +428,11 @@
     ).astype(jnp.bfloat16)
     projected = lax.all_to_all(projected, "tp", split_axis=0, concat_axis=1, tiled=True)
     residual = tokens.astype(jnp.float32) + rms_scale(projected, mix_gain)
-    expert_in = rms_scale(residual, ffn_gain).astype(jnp.bfloat16)
-    experts = lax.axis_size("ep")
-    hit = (routes[:, :, None] == lax.iota(jnp.int32, experts)[None, None, :]).astype(jnp.float32)
-    probs = jax.nn.softmax(route_logits, axis=-1)
-    combine = jnp.sum(probs[:, :, None] * hit, axis=1)
-    chosen = jnp.sum(hit, axis=1).T
-    outbound = jnp.dot(
-        chosen.astype(jnp.bfloat16), expert_in, preferred_element_type=jnp.float32
-    ).astype(jnp.bfloat16)[:, None, :]
-    slots = outbound.shape[1]
-    arrived = lax.all_to_all(outbound, "ep", split_axis=0, concat_axis=0, tiled=True)
-    flat = arrived.reshape(experts * slots, width)
-    pooled = lax.all_gather(flat, "tp", axis=0, tiled=True)
-    piece = pooled
-    gate = jnp.dot(piece, w_gate[0], preferred_element_type=jnp.float32) + gate_bias[0]
-    linear = jnp.dot(piece, w_lin[0], preferred_element_type=jnp.float32) + lin_bias[0]
-    act = clamped_unit(gate, linear).astype(jnp.bfloat16)
-    summed = lax.psum_scatter(
-        jnp.dot(act, w_down[0], preferred_element_type=jnp.float32).astype(jnp.bfloat16),
-        "tp",
-        scatter_dimension=0,
-        tiled=True,
-    )
-    returned = lax.all_to_all(
-        summed.reshape(experts, slots, width), "ep", split_axis=0, concat_axis=0, tiled=True
-    )
-    moe = jnp.einsum("se,ed->sd", combine, returned[:, 0, :].astype(jnp.float32))
-    updated = (residual + rms_scale(moe, post_gain)).astype(jnp.bfloat16)
-    return (updated, fresh)
+    updated = run_experts(
+        residual, ffn_gain[None, :], post_gain[None, :], routes, route_logits, gate_bias, lin_bias,
+        w_gate, w_lin, w_down,
+    )
+    return (updated.astype(BF16), fresh)
 
 
 def solution(mesh):

time: 221 us -> 122 us (0.55)
  waiting for transfers between devices: 120 us -> 12.8 us
  Pallas kernels: 0 us -> 58.3 us
  blocking collectives: 38.3 us -> 21.7 us
  between operations: 14.3 us -> 0.92 us
  matrix products: 11.8 us -> 4.53 us
  starting transfers between devices: 20.7 us -> 13.7 us
  other arithmetic: 9.53 us -> 5.2 us
    reduce_scatter x1 -> x0, waiting for transfers between devices: 59.5 us -> none  [per_device(): lax.psum_scatter(jnp.dot(act, w_down[0], preferred_element_type=jnp.float...]
    pallas_call x0 -> x1, Pallas kernels: none -> 58.3 us  [run_experts(): pl.pallas_call(expert_kernel, out_shape=jax.ShapeDtypeStruct((seqs, width...]
    all_gather x1 -> x0, waiting for transfers between devices: 33.5 us -> none  [per_device(): pooled = lax.all_gather(flat, 'tp', axis=0, tiled=True)]
    all_to_all x2, blocking collectives: 38.3 us -> 21.7 us  [the longest x1 12.1 us: sent_to_all(): return lax.all_to_all(copies, axis, split_axis=0, concat_axis=0, tiled=True)]
    all_to_all x2 -> x1, waiting for transfers between devices: 14.9 us -> 6 us  [sent_to_all(): return lax.all_to_all(copies, axis, split_axis=0, concat_axis=0, tiled=True)]
    dot_general x4 -> x0, matrix products: 6.89 us -> none  [the longest x1 3.81 us: per_device(): jnp.dot(act, w_down[0], preferred_element_type=jnp.float32)]
    all_to_all x1 -> x0, waiting for transfers between devices: 6.4 us -> none  [per_device(): lax.all_to_all(projected, 'tp', split_axis=0, concat_axis=1, tiled=True)]
    all_to_all x2 -> x1, starting transfers between devices: 13.8 us -> 10.1 us  [sent_to_all(): return lax.all_to_all(copies, axis, split_axis=0, concat_axis=0, tiled=True)]
  transfers between devices with their start and end apart: 6 -> 2, of which waited for: 6 -> 2; matrix products, arithmetic and copies ran while one was open for 2% -> 3% of each run, Pallas kernels for 0% -> 0%
where the time goes in v1:
time: 122 us; the launch traced here: 121 us
  Pallas kernels  58.3 us (48%)
  blocking collectives  21.7 us (18%)
  starting transfers between devices  13.7 us (11%)
  waiting for transfers between devices  12.8 us (10%)
  other arithmetic  5.2 us (4%)
  matrix products  4.53 us (4%)
  local copies, waits for them, and re-layouts  3.4 us (3%)
    pallas_call x1, Pallas kernels, run_experts(): pl.pallas_call(expert_kernel, out_shape=jax.ShapeDtypeStruct((seqs, width...  58.3 us
    all_to_all x1, blocking collectives, sent_to_all(): return lax.all_to_all(copies, axis, split_axis=0, concat_axis=0, tiled=True)  12.1 us
    all_to_all x1, starting transfers between devices, sent_to_all(): return lax.all_to_all(copies, axis, split_axis=0, concat_axis=0, tiled=True)  10.1 us
    all_to_all x1, blocking collectives, per_device(): lax.all_to_all(projected, 'tp', split_axis=0, concat_axis=1, tiled=True)  9.6 us
    all_to_all x1, waiting for transfers between devices, per_device(): lax.all_to_all(gathered, 'tp', split_axis=0, concat_axis=1, tiled=True)  6.8 us
    all_to_all x1, waiting for transfers between devices, sent_to_all(): return lax.all_to_all(copies, axis, split_axis=0, concat_axis=0, tiled=True)  6 us
    all_to_all x1, starting transfers between devices, per_device(): lax.all_to_all(gathered, 'tp', split_axis=0, concat_axis=1, tiled=True)  3.53 us
  transfers between devices with their start and end apart: 2, of which 2 were waited for; matrix products, arithmetic and copies ran while one was open for 3% of the time, Pallas kernels for 0%

profile of v1, /device:TPU:1, one launch (start us, length us, event | category | flops | bytes accessed | tf_op | source)
XLA Modules:
  0.0 120.5 jit_solution(4837375823852013163)
XLA Ops:
  0.6 0.0 copy-start
  0.6 0.0 copy-start.12
  0.7 0.0 copy-start.10
  0.7 0.9 fusion.21
  1.6 0.0 copy-done.12
  1.6 0.8 fusion.23
  2.4 0.7 broadcast_in_dim.58
  3.1 10.1 %all-to-all-start = ((bf16[16,2,2048]{2,1,0:T(2,128)(2,1)}), bf16[16,2,2048]{2,1,0:T(2,128)(2,1)S(1)}, u32[]{:S(2)}, u32[]{:S(2)}) async-start(bf16[16,2,2048]{2,1,0:T(2,128)(2,1)} %broadcast_in_dim.58), calls=%async_computation | async-start | bytes 262144 | tf_op jit(solution)/shard_map/all_to_all | solution.py:32
  13.3 0.7 broadcast_add_fusion
  13.9 0.1 iota_compare_fusion
  14.0 0.8 select_reduce_fusion
  14.8 0.8 fusion.30
  15.6 0.8 broadcast_subtract_fusion
  16.4 6.0 %all-to-all-done = bf16[16,2,2048]{2,1,0:T(2,128)(2,1)S(1)} async-done(((bf16[16,2,2048]{2,1,0:T(2,128)(2,1)}), bf16[16,2,2048]{2,1,0:T(2,128)(2,1)S(1)}, u32[]{:S(2)}, u32[]{:S(2)}) %all-to-all-start) | async-done | bytes 131104 | tf_op jit(solution)/shard_map/all_to_all | solution.py:32
  22.4 1.1 convolution_convert_fusion.1
  23.5 0.0 copy-done.10
  23.5 0.2 convolution_convert_fusion.2
  23.8 0.6 copy.34
  24.4 0.0 copy-start.15
  24.4 3.5 %all-to-all-start.1 = ((bf16[16,2,160]{2,1,0:T(2,128)(2,1)}), bf16[16,2,160]{2,1,0:T(2,128)(2,1)S(1)}, u32[]{:S(2)}, u32[]{:S(2)}) async-start(bf16[16,2,160]{2,1,0:T(2,128)(2,1)} %copy.34), calls=%async_computation.1 | async-start | bytes 32768 | tf_op jit(solution)/shard_map/all_to_all | solution.py:393
  27.9 0.0 copy-done.15
  27.9 0.1 iota_compare_fusion.1
  28.0 6.8 %all-to-all-done.1 = bf16[16,2,160]{2,1,0:T(2,128)(2,1)S(1)} async-done(((bf16[16,2,160]{2,1,0:T(2,128)(2,1)}), bf16[16,2,160]{2,1,0:T(2,128)(2,1)S(1)}, u32[]{:S(2)}, u32[]{:S(2)}) %all-to-all-start.1) | async-done | bytes 10272 | tf_op jit(solution)/shard_map/all_to_all | solution.py:393
  34.9 0.1 reshape.117
  34.9 0.0 copy-start.13
  34.9 0.6 copy-done.13
  35.5 0.1 fusion.24
  35.7 0.0 copy-done
  35.7 0.5 fusion.34
  36.1 0.2 fusion.13
  36.4 0.0 copy-start.11
  36.4 0.0 copy-start.3
  36.4 1.6 %fusion.3 = bf16[1,2,16,128]{3,2,1,0:T(8,128)(2,1)S(1)} fusion(f32[2,2,8,1024]{3,2,1,0:T(8,128)S(1)} %get-tuple-element.7, f32[2,2,8]{2,1,0:T(2,128)S(1)} %get-tuple-element.3, f32[2,2,8]{2,1,0:T(2,128)S(1)} %multiply_maximum_fusion, pred[2,1024]{1,0:T(4,128)(4,1)S(1)} %iota_compare_fusion.1, f32[2,2,128]{2,1,0:T(2,128)S(1)} %reshape.121, ...), kind=kOutput, calls=%fused_computation.8 | convolution fusion | flops 8531968 | bytes 1192320 | tf_op jit(solution)/shard_map/sgqp,spgd->sgqd/dot_general | solution.py:419
  38.0 0.1 broadcast_in_dim.63
  38.1 0.0 copy-start.2
  38.1 12.1 %all_to_all.36 = bf16[16,2,2048]{2,1,0:T(2,128)(2,1)S(1)} all-to-all(bf16[16,2,2048]{2,1,0:T(2,128)(2,1)S(1)} %broadcast_in_dim.63), channel_id=1, replica_groups=mesh['ep'=32,'tp'=16] {'tp'}, dimensions={0} | all-to-all | bytes 262144 | tf_op jit(solution)/shard_map/all_to_all | solution.py:32
  50.2 0.0 copy-start.1
  50.2 0.1 reshape.120
  50.3 0.0 copy-done.11
  50.3 0.2 convolution_convert_fusion
  50.5 0.0 copy-start.4
  50.5 0.0 copy-start.5
  50.5 0.0 copy-start.7
  50.5 0.0 copy-start.9
  50.6 9.6 %all_to_all.37 = bf16[16,2,128]{2,1,0:T(2,128)(2,1)S(1)} all-to-all(bf16[16,2,128]{2,1,0:T(2,128)(2,1)S(1)} %bitcast.61), channel_id=1, replica_groups=mesh['ep'=32,'tp'=16] {'tp'}, dimensions={0} | all-to-all | bytes 16384 | tf_op jit(solution)/shard_map/all_to_all | solution.py:429
  60.2 0.0 copy-start.14
  60.2 0.1 fusion.20
  60.3 0.6 copy-done.14
  60.9 0.1 convert_add_fusion.residual_ref
  60.9 0.0 copy-start.6
  60.9 0.0 copy-start.8
  60.9 0.0 copy-done.3
  61.0 0.0 copy-done.2
  61.0 0.0 copy-done.1
  61.0 0.0 copy-done.4
  61.0 0.0 copy-done.5
  61.0 0.0 copy-done.7
  61.0 0.0 copy-done.9
  61.0 0.6 copy-done.6
  61.6 0.0 copy-done.8
  61.6 58.3 %experts.1 = f32[2,2048]{1,0:T(2,128)S(1)} custom-call(f32[2,2048]{1,0:T(2,128)S(1)} %convert_add_fusion.residual_ref, f32[1,2048]{1,0:T(1,128)S(1)} %bitcast.56, f32[1,2048]{1,0:T(1,128)S(1)} %bitcast.57, s32[2,4]{1,0:T(2,128)S(1)} %copy-done.6, f32[2,4]{1,0:T(2,128)S(1)} %copy-done.7, f32[1,128]{1,0:T(1,128)S(1)} %copy-done.8, f32[1,128]{1,0:T(1,128)S(1)} %copy-done.9, ...), custom_call_target="tpu_custom_call" | custom-call | tf_op jit(solution)/shard_map/experts/pallas_call | solution.py:305
  119.9 0.6 convert_element_type.67
  (12 shorter events, 0.1 us)
Async XLA Ops:
  0.6 35.0 %copy-start = (bf16[2,1024,256]{2,1,0:T(8,128)(2,1)S(1)}, bf16[2,1024,256]{2,1,0:T(8,128)(2,1)}, u32[]{:S(2)}) copy-start(bf16[2,1024,256]{2,1,0:T(8,128)(2,1)} %param.22) | copy-start | bytes 3145732
  0.6 1.0 copy-start.12
  0.7 22.9 %copy-start.10 = (bf16[2048,128]{1,0:T(8,128)(2,1)S(1)}, bf16[2048,128]{1,0:T(8,128)(2,1)}, u32[]{:S(2)}) copy-start(bf16[2048,128]{1,0:T(8,128)(2,1)} %param.29) | copy-start | bytes 1572868
  3.1 19.3 %all-to-all-start = ((bf16[16,2,2048]{2,1,0:T(2,128)(2,1)}), bf16[16,2,2048]{2,1,0:T(2,128)(2,1)S(1)}, u32[]{:S(2)}, u32[]{:S(2)}) async-start(bf16[16,2,2048]{2,1,0:T(2,128)(2,1)} %broadcast_in_dim.58), calls=%async_computation | async-start | bytes 262144 | tf_op jit(solution)/shard_map/all_to_all | solution.py:32
  24.4 3.5 %copy-start.15 = (s32[2]{0:T(128)S(1)}, s32[2]{0:T(128)}, u32[]{:S(2)}) copy-start(s32[2]{0:T(128)} %param.25) | copy-start | bytes 28
  24.4 10.4 %all-to-all-start.1 = ((bf16[16,2,160]{2,1,0:T(2,128)(2,1)}), bf16[16,2,160]{2,1,0:T(2,128)(2,1)S(1)}, u32[]{:S(2)}, u32[]{:S(2)}) async-start(bf16[16,2,160]{2,1,0:T(2,128)(2,1)} %copy.34), calls=%async_computation.1 | async-start | bytes 32768 | tf_op jit(solution)/shard_map/all_to_all | solution.py:393
  34.9 0.6 copy-start.13
  36.4 13.9 %copy-start.11 = (bf16[2048,128]{1,0:T(8,128)(2,1)S(1)}, bf16[2048,128]{1,0:T(8,128)(2,1)}, u32[]{:S(2)}) copy-start(bf16[2048,128]{1,0:T(8,128)(2,1)} %param.33) | copy-start | bytes 1572868
  36.4 24.6 %copy-start.3 = (bf16[1,128,2048]{2,1,0:T(8,128)(2,1)S(1)}, bf16[1,128,2048]{2,1,0:T(8,128)(2,1)}, u32[]{:S(2)}) copy-start(bf16[1,128,2048]{2,1,0:T(8,128)(2,1)} %w_down_hbm.1) | copy-start | bytes 1572868
  38.1 22.9 %copy-start.2 = (bf16[1,2048,128]{2,1,0:T(8,128)(2,1)S(1)}, bf16[1,2048,128]{2,1,0:T(8,128)(2,1)}, u32[]{:S(2)}) copy-start(bf16[1,2048,128]{2,1,0:T(8,128)(2,1)} %w_lin_hbm.1) | copy-start | bytes 1572868
  50.2 10.7 %copy-start.1 = (bf16[1,2048,128]{2,1,0:T(8,128)(2,1)S(1)}, bf16[1,2048,128]{2,1,0:T(8,128)(2,1)}, u32[]{:S(2)}) copy-start(bf16[1,2048,128]{2,1,0:T(8,128)(2,1)} %w_gate_hbm.1) | copy-start | bytes 1572868
  50.5 10.5 %copy-start.4 = (f32[2048]{0:T(1024)S(1)}, f32[2048]{0:T(1024)}, u32[]{:S(2)}) copy-start(f32[2048]{0:T(1024)} %param.35) | copy-start | bytes 24580
  50.5 10.5 %copy-start.5 = (f32[2048]{0:T(1024)S(1)}, f32[2048]{0:T(1024)}, u32[]{:S(2)}) copy-start(f32[2048]{0:T(1024)} %param.41) | copy-start | bytes 24580
  50.5 10.5 %copy-start.7 = (f32[2,4]{1,0:T(2,128)S(1)}, f32[2,4]{1,0:T(2,128)}, u32[]{:S(2)}) copy-start(f32[2,4]{1,0:T(2,128)} %logits_ref.1) | copy-start | bytes 100
  50.5 10.5 %copy-start.9 = (f32[1,128]{1,0:T(1,128)S(1)}, f32[1,128]{1,0:T(1,128)}, u32[]{:S(2)}) copy-start(f32[1,128]{1,0:T(1,128)} %lin_bias_ref.1) | copy-start | bytes 1540
  60.2 0.7 copy-start.14
  60.9 0.7 copy-start.6
  60.9 0.7 copy-start.8

commit v2 on v1

v2 whole, which is shorter than its diff:
```python
import functools
from types import SimpleNamespace

import jax
import jax.numpy as jnp
from jax import lax
from jax.experimental import pallas as pl
from jax.experimental.pallas import tpu as pltpu
from jax.sharding import PartitionSpec as P

HEADS = 16
KVH = 2
HDIM = 128

NORM_EPS = 1e-06
SWIGLU_ALPHA = 1.702
SWIGLU_LIMIT = 7.0
NEG_LARGE = -1e30
MESH = pl.DeviceIdType.MESH
CORES = 2
F32 = jnp.float32
BF16 = jnp.bfloat16


def rms_scale(values, gain):
    values = values.astype(F32)
    return values * lax.rsqrt(jnp.mean(values * values, axis=-1, keepdims=True) + NORM_EPS) * gain


def clamped_unit(gate, linear):
    gate = jnp.minimum(gate, SWIGLU_LIMIT)
    linear = jnp.clip(linear, -SWIGLU_LIMIT, SWIGLU_LIMIT)
    return gate * jax.nn.sigmoid(SWIGLU_ALPHA * gate) * (linear + 1.0)


def goes(way, chunk, reach, half):
    return 1 <= reach <= (half if way == chunk else half - 1)


def remote(src, dst, send_sem, recv_sem, to):
    return pltpu.make_async_remote_copy(
        src_ref=src, dst_ref=dst, send_sem=send_sem, recv_sem=recv_sem,
        device_id=to, device_id_type=MESH,
    )


def arrived(ref, sem):
    pltpu.make_async_copy(ref, ref, sem).wait()


def split_rows(row):
    half = row.shape[1] // 2
    return jnp.concatenate([row[:, :half], row[:, half:]], axis=0)


INPUTS = (
    "tokens", "lengths", "routes", "logits", "attn_gain", "forget_bias", "w_forget", "mix_gain",
    "ffn_gain", "post_gain", "gate_bias", "lin_bias", "keys_hbm", "values_hbm", "gates_hbm",
    "w_query_hbm", "w_keyval_hbm", "w_out_hbm", "w_gate_hbm", "w_lin_hbm", "w_down_hbm",
)
OUTPUTS = ("updated", "fresh")
SCRATCH = (
    "keys", "values", "gates", "w_query", "w_keyval", "w_out", "w_in", "w_down",
    "normed_out", "normed_in", "qkv_out", "qkv_in", "mixed_rows", "mixed_out", "mixed_in",
    "proj_out", "proj_in",
    "outbox", "inbox", "rows", "parts", "peer_parts", "ring_in", "ring_out", "back_out", "back_in",
    "load_sem", "normed_send", "normed_recv", "qkv_send", "qkv_recv", "mixed_send", "mixed_recv",
    "proj_send", "proj_recv",
    "go_send", "go_recv", "cw_send", "ccw_send", "core_send", "ring_recv", "core_recv",
    "part_send", "part_recv", "sum_send", "sum_recv", "back_send", "back_recv",
)


def layer_kernel(*refs):
    r = SimpleNamespace(**dict(zip(INPUTS + OUTPUTS + SCRATCH, refs, strict=True)))
    eps = lax.axis_size("ep")
    tps = lax.axis_size("tp")
    ny = tps // CORES
    half = ny // 2
    seqs, width = r.tokens.shape
    hidden = r.w_down.shape[0]
    chunk_rows = eps // 2
    me_ep = lax.axis_index("ep")
    me_tp = lax.axis_index("tp")
    me_y = me_tp // CORES
    me_c = me_tp % CORES

    def at(shift, core=None):
        core = me_c if core is None else core
        return {"tp": lax.rem(me_y + shift + ny, ny) * CORES + core}

    partner = at(0, 1 - me_c)

    pairs_to_load = {
        "query": (r.w_query_hbm, r.w_query),
        "keyval": (r.w_keyval_hbm, r.w_keyval),
        "keys": (r.keys_hbm, r.keys),
        "gates": (r.gates_hbm, r.gates),
        "values": (r.values_hbm, r.values),
        "out": (r.w_out_hbm, r.w_out),
        "gate": (r.w_gate_hbm.at[0], r.w_in.at[:, pl.ds(0, hidden)]),
        "lin": (r.w_lin_hbm.at[0], r.w_in.at[:, pl.ds(hidden, hidden)]),
        "down": (r.w_down_hbm.at[0], r.w_down),
    }

    barrier = pltpu.get_barrier_semaphore()
    far_first = sorted(range(1, eps), key=lambda d: -min(d, eps - d))
    peers = [
        (shift, core)
        for shift in sorted(range(ny), key=lambda d: -min(d, ny - d))
        for core in ((0, 1) if shift else (1,))
    ]

    def peer(shift, core):
        return lax.rem(me_y + shift, ny) * CORES + lax.rem(me_c + core, CORES)

    for d in far_first:
        to = {"ep": lax.rem(me_ep + d, eps)}
        pl.semaphore_signal(barrier, inc=1, device_id=to, device_id_type=MESH)
    for shift, core in peers:
        to = {"tp": peer(shift, core)}
        pl.semaphore_signal(barrier, inc=1, device_id=to, device_id_type=MESH)

    loads = {
        name: pltpu.make_async_copy(src, dst, r.load_sem.at[i])
        for i, (name, (src, dst)) in enumerate(pairs_to_load.items())
    }
    for load in loads.values():
        load.start()

    tokens = r.tokens[...].astype(F32)
    normed = rms_scale(tokens, r.attn_gain[...]).astype(BF16)
    r.normed_out[...] = normed

    pl.semaphore_wait(barrier, eps - 1 + tps - 1)

    def to_group(outbox_of, inbox, send, recv):
        for shift, core in peers:
            to = peer(shift, core)
            remote(outbox_of(to), inbox.at[me_tp], send, recv, {"tp": to}).start()
        pltpu.make_async_copy(outbox_of(me_tp), inbox.at[me_tp], recv).start()

    to_group(lambda to: r.normed_out, r.normed_in, r.normed_send, r.normed_recv)
    forget = jnp.concatenate(
        [
            jnp.sum(normed.astype(F32) * r.w_forget[g : g + 1, :].astype(F32), axis=1, keepdims=True)
            for g in range(KVH)
        ],
        axis=1,
    ) + r.forget_bias[...]
    forget = jnp.minimum(forget, 0.0) - jnp.log1p(jnp.exp(-jnp.abs(forget)))

    loads["query"].wait()
    loads["keyval"].wait()
    arrived(r.normed_in, r.normed_recv)
    piece = jnp.concatenate([r.normed_in[i].astype(F32) for i in range(tps)], axis=0).astype(BF16)
    query = jnp.dot(piece, r.w_query[...], preferred_element_type=F32)
    keyval = lax.dot_general(
        piece, r.w_keyval[...], (((1,), (1,)), ((), ())), preferred_element_type=F32
    )
    pair_cols = keyval.shape[1]
    both = jnp.concatenate(
        [query, keyval, jnp.zeros((seqs * tps, HDIM - pair_cols), F32)], axis=1
    )
    for i in range(tps):
        r.qkv_out[i] = both[seqs * i : seqs * (i + 1), :].astype(BF16)
    to_group(lambda to: r.qkv_out.at[to], r.qkv_in, r.qkv_send, r.qkv_recv)

    group = HEADS // KVH
    span = r.keys.shape[1]
    scale = HDIM ** (-0.5)
    head = lax.broadcasted_iota(jnp.int32, (HEADS, 1), 0)
    lower = head < group
    place = lax.broadcasted_iota(jnp.int32, (HEADS, span), 1)
    loads["keys"].wait()
    loads["gates"].wait()
    loads["values"].wait()
    arrived(r.qkv_in, r.qkv_recv)
    per_tile = HDIM // pair_cols
    fresh_rows = []
    for s in range(seqs):
        mine = jnp.concatenate([r.qkv_in[j].astype(F32)[s : s + 1, :] for j in range(tps)], axis=0)
        q = mine[:, :HDIM]
        kv = mine[:, HDIM:]
        spread = kv
        for i in range(1, per_tile):
            spread = jnp.where(head % per_tile == i, pltpu.roll(kv, i * pair_cols, 1), spread)
        tiles = [
            jnp.sum(spread[per_tile * b : per_tile * (b + 1), :], axis=0, keepdims=True)
            for b in range(2 * KVH)
        ]
        fresh_rows.append(jnp.concatenate(tiles, axis=1))
        new_key = jnp.where(lower, tiles[0], tiles[1])
        new_value = jnp.where(lower, tiles[2], tiles[3])
        gates = jnp.where(lower, r.gates[s, 0:1, :], r.gates[s, 1:2, :])
        length = r.lengths[s]
        last = jnp.sum(jnp.where(place == length - 1, gates, 0.0), axis=1, keepdims=True)
        base = last + jnp.where(lower, forget[s : s + 1, 0:1], forget[s : s + 1, 1:2])
        own = jnp.sum(q * new_key, axis=1, keepdims=True) * scale
        q_wide = jnp.concatenate([jnp.where(lower, q, 0.0), jnp.where(lower, 0.0, q)], axis=1)
        score = lax.dot_general(
            q_wide.astype(BF16), r.keys[s], (((1,), (1,)), ((), ())), preferred_element_type=F32
        )
        live = place < length
        masked = jnp.where(live, score * scale + (base - gates), NEG_LARGE)
        top = jnp.maximum(jnp.max(masked, axis=1, keepdims=True), own)
        expo = jnp.where(live, jnp.exp(masked - top), 0.0)
        own_expo = jnp.exp(own - top)
        total = jnp.sum(expo, axis=1, keepdims=True) + own_expo
        weights = (expo / total).astype(BF16)
        own_weight = (own_expo / total).astype(BF16).astype(F32)
        mixed = jnp.dot(weights, r.values[s], preferred_element_type=F32)
        mixed = jnp.where(lower, mixed[:, :HDIM], mixed[:, HDIM:]) + own_weight * new_value
        for h in range(HEADS):
            r.mixed_rows[s : s + 1, h * HDIM : (h + 1) * HDIM] = mixed[h : h + 1, :]
    r.mixed_out[...] = r.mixed_rows[...].astype(BF16)
    to_group(lambda to: r.mixed_out, r.mixed_in, r.mixed_send, r.mixed_recv)
    r.fresh[...] = jnp.concatenate(fresh_rows, axis=0).astype(BF16)

    loads["out"].wait()
    arrived(r.mixed_in, r.mixed_recv)
    piece = jnp.concatenate([r.mixed_in[i].astype(F32) for i in range(tps)], axis=0).astype(BF16)
    projected = jnp.dot(piece, r.w_out[...], preferred_element_type=F32)
    for i in range(tps):
        r.proj_out[i] = projected[seqs * i : seqs * (i + 1), :].astype(BF16)
    to_group(lambda to: r.proj_out.at[to], r.proj_in, r.proj_send, r.proj_recv)
    arrived(r.proj_in, r.proj_recv)
    projected = jnp.concatenate([r.proj_in[j].astype(F32) for j in range(tps)], axis=1)
    residual = tokens + rms_scale(projected, r.mix_gain[...])

    expert_in = rms_scale(residual, r.ffn_gain[...]).astype(BF16).astype(F32)
    routes = r.routes[...]
    top = routes.shape[1]
    entry = lax.broadcasted_iota(jnp.int32, (2 * eps, 1), 0)
    owner, side = entry // 2, entry % 2
    hw = width // 2
    mail = jnp.zeros((2 * eps, hw), F32)
    for s in range(seqs):
        named = functools.reduce(
            jnp.logical_or, [owner == routes[s : s + 1, k : k + 1] for k in range(top)]
        )
        row = expert_in[s : s + 1, :]
        mail = jnp.where(named & (side == 0), row[:, :hw], mail)
        mail = jnp.where(named & (side == 1), row[:, hw:], mail)
    for e in range(eps):
        r.outbox[e] = mail[2 * e : 2 * e + 2, :].astype(BF16)

    for d in far_first:
        to = lax.rem(me_ep + d, eps)
        remote(
            r.outbox.at[to], r.inbox.at[me_ep], r.go_send, r.go_recv.at[me_ep // chunk_rows], {"ep": to}
        ).start()
    pltpu.make_async_copy(
        r.outbox.at[me_ep], r.inbox.at[me_ep], r.go_recv.at[me_ep // chunk_rows]
    ).start()

    probs = jax.nn.softmax(r.logits[...], axis=-1)
    lane = lax.broadcasted_iota(jnp.int32, (seqs, eps), 1)
    combine = jnp.zeros((seqs, eps), F32)
    for k in range(top):
        combine += jnp.where(routes[:, k : k + 1] == lane, probs[:, k : k + 1], 0.0)

    def shift_of(slot):
        if slot == 0:
            return 0
        return -slot if slot <= half else slot - half

    def chip(slot):
        return lax.rem(me_y + shift_of(slot) + ny, ny)

    sends = []

    def pass_on(slot, g):
        block = r.rows.at[chip(slot), me_c, g]
        if slot == 0:
            ways = [(0, 1), (1, 1)]
        else:
            ways = [(0, slot + 1)] if slot <= half else [(1, slot - half + 1)]
        for way, reach in ways:
            if goes(way, g, reach, half):
                there = reach if way == 0 else half + reach
                sends.append(remote(
                    block, block, (r.cw_send if way == 0 else r.ccw_send).at[slot, g],
                    r.ring_recv.at[there, g], at(1 if way == 0 else -1),
                ))
                sends[-1].start()
        sends.append(remote(block, block, r.core_send.at[slot, g], r.core_recv.at[slot, g], partner))
        sends[-1].start()

    for g in range(2):
        first = g * chunk_rows
        arrived(r.inbox.at[pl.ds(first, chunk_rows)], r.go_recv.at[g])
        pairs = [r.inbox[first + i].astype(F32) for i in range(chunk_rows)]
        r.rows[me_y, me_c, g] = jnp.concatenate(
            [
                jnp.concatenate([pair[0:1] for pair in pairs], axis=0),
                jnp.concatenate([pair[1:2] for pair in pairs], axis=0),
            ],
            axis=1,
        ).astype(BF16)
        pass_on(0, g)

    def slots_at(reach):
        if reach == 0:
            return [(0, (0, 1))]
        found = []
        for way in range(2):
            gs = tuple(g for g in range(2) if goes(way, g, reach, half))
            if gs:
                found.append((reach if way == 0 else half + reach, gs))
        return found

    def work(reach):
        slots = slots_at(reach)
        for slot, gs in slots:
            for g in gs:
                block = r.rows.at[chip(slot), 1 - me_c, g]
                arrived(block, r.core_recv.at[slot, g])
        for slot in [slots[0][0]] if reach == half else [slot for slot, _ in slots]:
            place = chip(slot)
            x = r.rows[place].reshape(4 * chunk_rows, width)
            both = jnp.dot(x, r.w_in[...], preferred_element_type=F32)
            act = clamped_unit(
                both[:, :hidden] + r.gate_bias[...], both[:, hidden:] + r.lin_bias[...]
            ).astype(BF16)
            out = jnp.dot(act, r.w_down[...], preferred_element_type=F32).astype(BF16)
            r.parts[place] = out.reshape(2, 2, chunk_rows, width)
            sends.append(remote(
                r.parts.at[place, 1 - me_c], r.peer_parts.at[place], r.part_send.at[slot],
                r.part_recv.at[slot], partner,
            ))
            sends[-1].start()

    for name in ("gate", "lin", "down"):
        loads[name].wait()
    for reach in range(1, half + 1):
        for slot, gs in sorted(slots_at(reach), key=lambda pair: pair[1]):
            for g in gs:
                arrived(r.rows.at[chip(slot), me_c, g], r.ring_recv.at[slot, g])
                pass_on(slot, g)
        work(reach - 1)
    work(half)

    seen = set()

    def local_sum(slot, g):
        place = chip(slot)
        if slot not in seen:
            arrived(r.peer_parts.at[place], r.part_recv.at[slot])
            seen.add(slot)
        return r.parts[place, me_c, g].astype(F32) + r.peer_parts[place, g].astype(F32)

    def inward(way, reach, g):
        arrived(r.ring_in.at[way, reach, g], r.sum_recv.at[way, reach, g])
        return r.ring_in[way, reach, g].astype(F32)

    for reach in range(half, 0, -1):
        for way, g in [(0, 1), (1, 0), (0, 0), (1, 1)]:
            if not goes(way, g, reach, half):
                continue
            slot = half if reach == half else (half + reach if way == 0 else reach)
            total = local_sum(slot, g)
            if goes(way, g, reach + 1, half):
                total += inward(way, reach + 1, g)
            r.ring_out[way, reach, g] = total.astype(BF16)
            sends.append(remote(
                r.ring_out.at[way, reach, g], r.ring_in.at[way, reach, g],
                r.sum_send.at[way, reach, g], r.sum_recv.at[way, reach, g],
                at(1 if way == 0 else -1),
            ))
            sends[-1].start()

    for g in range(2):
        total = local_sum(0, g)
        for way in range(2):
            if goes(way, g, 1, half):
                total += inward(way, 1, g)
        for i in range(chunk_rows):
            r.back_out[g * chunk_rows + i] = split_rows(total[i : i + 1, :]).astype(BF16)
        for i in range(chunk_rows):
            to = g * chunk_rows + i

            @pl.when(me_ep != to)
            def _():
                remote(
                    r.back_out.at[to], r.back_in.at[me_ep], r.back_send, r.back_recv, {"ep": to}
                ).start()

            @pl.when(me_ep == to)
            def _():
                pltpu.make_async_copy(r.back_out.at[to], r.back_in.at[me_ep], r.back_recv).start()

    arrived(r.back_in, r.back_recv)
    finished = []
    for s in range(seqs):
        moe = jnp.zeros((2, hw), F32)
        for e in range(eps):
            moe += combine[s : s + 1, e : e + 1] * r.back_in[e].astype(F32)
        mean = jnp.sum(jnp.sum(moe * moe, axis=1, keepdims=True), axis=0, keepdims=True) / width
        moe = moe * lax.rsqrt(mean + NORM_EPS) * split_rows(r.post_gain[...])
        moe = jnp.concatenate([moe[0:1], moe[1:2]], axis=1)
        finished.append(residual[s : s + 1, :] + moe)
    r.updated[...] = jnp.concatenate(finished, axis=0).astype(BF16)

    for send in sends:
        send.wait_send()
    arrived(r.normed_in.at[pl.ds(0, tps - 1)], r.normed_send)
    arrived(r.mixed_in.at[pl.ds(0, tps - 1)], r.mixed_send)
    arrived(r.qkv_out.at[pl.ds(0, tps - 1)], r.qkv_send)
    arrived(r.proj_out.at[pl.ds(0, tps - 1)], r.proj_send)
    arrived(r.outbox.at[pl.ds(0, eps - 1)], r.go_send)
    arrived(r.back_out.at[pl.ds(0, eps - 1)], r.back_send)


def per_device(
    tokens, cache_keys, cache_values, cache_gates, lengths, routes, route_logits, attn_gain,
    w_query, w_keyval, w_forget, forget_bias, w_out, mix_gain, ffn_gain, w_gate, w_lin, gate_bias,
    lin_bias, w_down, post_gain,
):
    eps = lax.axis_size("ep")
    tps = lax.axis_size("tp")
    ny = tps // CORES
    half = ny // 2
    seqs, width = tokens.shape
    span = cache_keys.shape[1]
    hidden = w_down.shape[1]
    cols = w_query.shape[1]
    pair_cols = w_keyval.shape[1]
    r = eps // 2
    slots = 2 * half + 1
    vmem = pl.BlockSpec(memory_space=pltpu.VMEM)
    smem = pl.BlockSpec(memory_space=pltpu.SMEM)
    anyspace = pl.BlockSpec(memory_space=pl.ANY)
    dma = pltpu.SemaphoreType.DMA
    scratch = dict(
        keys=pltpu.VMEM(cache_keys.shape, BF16),
        values=pltpu.VMEM(cache_values.shape, BF16),
        gates=pltpu.VMEM(cache_gates.shape, F32),
        w_query=pltpu.VMEM((width, cols), BF16),
        w_keyval=pltpu.VMEM((pair_cols, width), BF16),
        w_out=pltpu.VMEM((width, cols), BF16),
        w_in=pltpu.VMEM((width, 2 * hidden), BF16),
        w_down=pltpu.VMEM((hidden, width), BF16),
        normed_out=pltpu.VMEM((seqs, width), BF16),
        normed_in=pltpu.VMEM((tps, seqs, width), BF16),
        qkv_out=pltpu.VMEM((tps, seqs, 2 * HDIM), BF16),
        qkv_in=pltpu.VMEM((tps, seqs, 2 * HDIM), BF16),
        mixed_rows=pltpu.VMEM((seqs, width), F32),
        mixed_out=pltpu.VMEM((seqs, width), BF16),
        mixed_in=pltpu.VMEM((tps, seqs, width), BF16),
        proj_out=pltpu.VMEM((tps, seqs, cols), BF16),
        proj_in=pltpu.VMEM((tps, seqs, cols), BF16),
        outbox=pltpu.VMEM((eps, 2, width // 2), BF16),
        inbox=pltpu.VMEM((eps, 2, width // 2), BF16),
        rows=pltpu.VMEM((ny, 2, 2, r, width), BF16),
        parts=pltpu.VMEM((ny, 2, 2, r, width), BF16),
        peer_parts=pltpu.VMEM((ny, 2, r, width), BF16),
        ring_in=pltpu.VMEM((2, half + 1, 2, r, width), BF16),
        ring_out=pltpu.VMEM((2, half + 1, 2, r, width), BF16),
        back_out=pltpu.VMEM((eps, 2, width // 2), BF16),
        back_in=pltpu.VMEM((eps, 2, width // 2), BF16),
        load_sem=dma((9,)),
        normed_send=dma, normed_recv=dma, qkv_send=dma, qkv_recv=dma,
        mixed_send=dma, mixed_recv=dma, proj_send=dma, proj_recv=dma,
        go_send=dma, go_recv=dma((2,)),
        cw_send=dma((slots, 2)), ccw_send=dma((slots, 2)), core_send=dma((slots, 2)),
        ring_recv=dma((slots, 2)), core_recv=dma((slots, 2)),
        part_send=dma((slots,)), part_recv=dma((slots,)),
        sum_send=dma((2, half + 1, 2)), sum_recv=dma((2, half + 1, 2)),
        back_send=dma, back_recv=dma,
    )
    operands = dict(
        tokens=tokens, lengths=lengths, routes=routes, logits=route_logits,
        attn_gain=attn_gain[None, :], forget_bias=forget_bias[None, :], w_forget=w_forget.T,
        mix_gain=mix_gain[None, :], ffn_gain=ffn_gain[None, :], post_gain=post_gain[None, :],
        gate_bias=gate_bias, lin_bias=lin_bias, keys_hbm=cache_keys, values_hbm=cache_values,
        gates_hbm=cache_gates, w_query_hbm=w_query, w_keyval_hbm=w_keyval.T, w_out_hbm=w_out,
        w_gate_hbm=w_gate, w_lin_hbm=w_lin, w_down_hbm=w_down,
    )
    spaces = [
        anyspace if name.endswith("_hbm") else smem if name == "lengths" else vmem
        for name in INPUTS
    ]
    return pl.pallas_call(
        layer_kernel,
        out_shape=(
            jax.ShapeDtypeStruct((seqs, width), BF16),
            jax.ShapeDtypeStruct((seqs, 2 * KVH * HDIM), BF16),
        ),
        in_specs=spaces,
        out_specs=(vmem, vmem),
        scratch_shapes=[scratch[name] for name in SCRATCH],
        compiler_params=pltpu.CompilerParams(
            collective_id=0, has_side_effects=True, vmem_limit_bytes=48 * 1024 * 1024
        ),
        name="layer",
    )(*[operands[name] for name in INPUTS])


def solution(mesh):
    in_specs = (
        P(("ep", "tp"), None),
        P(("ep", "tp"), None, None),
        P(("ep", "tp"), None, None),
        P(("ep", "tp"), None, None),
        P(("ep", "tp")),
        P(("ep", "tp"), None),
        P(("ep", "tp"), None),
        P(),
        P(None, "tp"),
        P(None, "tp"),
        P(),
        P(),
        P(None, "tp"),
        P(),
        P(),
        P("ep", None, "tp"),
        P("ep", None, "tp"),
        P("ep", "tp"),
        P("ep", "tp"),
        P("ep", "tp", None),
        P(),
    )
    out_specs = (P(("ep", "tp"), None), P(("ep", "tp"), None))
    return jax.shard_map(
        per_device, mesh=mesh, in_specs=in_specs, out_specs=out_specs, check_vma=False
    )
```

time: 122 us -> 103 us (0.84)
  Pallas kernels: 58.3 us -> 85.8 us
  blocking collectives: 21.7 us -> 0 us
  starting transfers between devices: 13.7 us -> 0 us
  waiting for transfers between devices: 12.8 us -> 0 us
  local copies, waits for them, and re-layouts: 3.4 us -> 14.6 us
  other arithmetic: 5.2 us -> 0 us
  matrix products: 4.53 us -> 0 us
    pallas_call x1, Pallas kernels: 58.3 us -> 85.8 us  [per_device(): pl.pallas_call(layer_kernel, out_shape=(jax.ShapeDtypeStruct((seqs, width...]
    all_to_all x2 -> x0, blocking collectives: 21.7 us -> none  [the longest x1 12.1 us: sent_to_all(): return lax.all_to_all(copies, axis, split_axis=0, concat_axis=0, tiled=True)]
    all_to_all x2 -> x0, starting transfers between devices: 13.7 us -> none  [the longest x1 10.1 us: sent_to_all(): return lax.all_to_all(copies, axis, split_axis=0, concat_axis=0, tiled=True)]
    unnamed x33 -> x44, local copies, waits for them, and re-layouts: 1.81 us -> 14.6 us
    all_to_all x2 -> x0, waiting for transfers between devices: 12.8 us -> none  [the longest x1 6.8 us: per_device(): lax.all_to_all(gathered, 'tp', split_axis=0, concat_axis=1, tiled=True)]
    dot_general x7 -> x0, matrix products: 4.53 us -> none  [the longest x1 1.62 us: per_device(): jnp.einsum('sgqp,spgd->sgqd', weights, values_four, preferred_element_typ...]
    reduce_sum x4 -> x0, other arithmetic: 2.08 us -> none  [the longest x2 1.07 us: rms_scale(): jnp.mean(values * values, axis=-1, keepdims=True) + NORM_EPS]
    sub x2 -> x0, other arithmetic: 1.46 us -> none  [the longest x1 0.8 us: block_scores(): scores = scores + (base[:, :, None, None] - cache_gates[:, :, None, :])]
  transfers between devices with their start and end apart: 2 -> 0, of which waited for: 2 -> 0; matrix products, arithmetic and copies ran while one was open for 3% -> 0% of each run, Pallas kernels for 0% -> 0%
where the time goes in v2:
time: 103 us; the launch traced here: 101 us
  Pallas kernels  85.8 us (83%)
  local copies, waits for them, and re-layouts  14.6 us (14%)
    pallas_call x1, Pallas kernels, per_device(): pl.pallas_call(layer_kernel, out_shape=(jax.ShapeDtypeStruct((seqs, width...  85.8 us
    unnamed x44, local copies, waits for them, and re-layouts  14.6 us

profile of v2, /device:TPU:1, one launch (start us, length us, event | category | flops | bytes accessed | tf_op | source)
XLA Modules:
  0.0 101.1 jit_solution(18113188468956506765)
XLA Ops:
  0.6 0.0 copy-start.9
  0.6 0.0 copy-start.20
  0.7 0.0 copy-start.16
  0.7 0.0 copy-start.18
  0.7 0.0 copy-start.19
  0.7 0.0 copy-start.15
  0.7 0.0 copy-start.17
  0.7 0.6 copy-done.9
  1.3 0.0 copy-done.20
  1.3 0.0 copy-done.16
  1.4 0.0 copy-done.18
  1.4 0.0 copy-done.19
  1.4 0.0 copy-done.15
  1.4 0.0 copy-done.17
  1.4 0.0 copy-start
  1.4 1.2 %copy-done = bf16[2,1024,256]{2,1,0:T(8,128)(2,1)S(1)} copy-done((bf16[2,1024,256]{2,1,0:T(8,128)(2,1)S(1)}, bf16[2,1024,256]{2,1,0:T(8,128)(2,1)}, u32[]{:S(2)}) %copy-start) | copy-done | bytes 1048600
  2.6 0.0 copy-start.1
  2.6 1.2 %copy-done.1 = bf16[2,1024,256]{2,1,0:T(8,128)(2,1)S(1)} copy-done((bf16[2,1024,256]{2,1,0:T(8,128)(2,1)S(1)}, bf16[2,1024,256]{2,1,0:T(8,128)(2,1)}, u32[]{:S(2)}) %copy-start.1) | copy-done | bytes 1048600
  3.9 0.0 copy-start.2
  3.9 1.0 %copy-done.2 = bf16[2048,128]{1,0:T(8,128)(2,1)S(1)} copy-done((bf16[2048,128]{1,0:T(8,128)(2,1)S(1)}, bf16[2048,128]{1,0:T(8,128)(2,1)}, u32[]{:S(2)}) %copy-start.2) | copy-done | bytes 524312
  4.9 0.0 copy-start.3
  4.9 1.0 %copy-done.3 = bf16[2048,128]{1,0:T(8,128)(2,1)S(1)} copy-done((bf16[2048,128]{1,0:T(8,128)(2,1)S(1)}, bf16[2048,128]{1,0:T(8,128)(2,1)}, u32[]{:S(2)}) %copy-start.3) | copy-done | bytes 524312
  5.9 0.0 copy-start.4
  5.9 1.0 %copy-done.4 = bf16[1,2048,128]{2,1,0:T(8,128)(2,1)S(1)} copy-done((bf16[1,2048,128]{2,1,0:T(8,128)(2,1)S(1)}, bf16[1,2048,128]{2,1,0:T(8,128)(2,1)}, u32[]{:S(2)}) %copy-start.4) | copy-done | bytes 524312
  7.0 0.0 copy-start.5
  7.0 1.0 %copy-done.5 = bf16[1,2048,128]{2,1,0:T(8,128)(2,1)S(1)} copy-done((bf16[1,2048,128]{2,1,0:T(8,128)(2,1)S(1)}, bf16[1,2048,128]{2,1,0:T(8,128)(2,1)}, u32[]{:S(2)}) %copy-start.5) | copy-done | bytes 524312
  8.0 0.0 copy-start.6
  8.0 1.0 %copy-done.6 = bf16[1,128,2048]{2,1,0:T(8,128)(2,1)S(1)} copy-done((bf16[1,128,2048]{2,1,0:T(8,128)(2,1)S(1)}, bf16[1,128,2048]{2,1,0:T(8,128)(2,1)}, u32[]{:S(2)}) %copy-start.6) | copy-done | bytes 524312
  9.1 0.0 copy-start.7
  9.1 0.9 copy-done.7
  10.0 0.0 copy-start.8
  10.0 0.7 copy-done.8
  10.7 0.0 copy-start.10
  10.7 0.7 copy-done.10
  11.4 0.0 copy-start.11
  11.4 0.7 copy-done.11
  12.1 0.0 copy-start.12
  12.1 0.7 copy-done.12
  12.8 0.0 copy-start.13
  12.8 0.7 copy-done.13
  13.5 0.0 copy-start.14
  13.5 0.7 copy-done.14
  14.2 85.8 %layer.1 = (bf16[2,2048]{1,0:T(2,128)(2,1)S(1)}, bf16[2,512]{1,0:T(2,128)(2,1)S(1)}) custom-call(bf16[2,2048]{1,0:T(2,128)(2,1)S(1)} %copy-done.9, s32[2]{0:T(128)S(1)} %copy-done.17, s32[2,4]{1,0:T(2,128)S(1)} %copy-done.15, f32[2,4]{1,0:T(2,128)S(1)} %copy-done.16, f32[1,2048]{1,0:T(1,128)S(1)} %bitcast.8, f32[1,2]{1,0:T(1,128)S(1)} %bitcast.13, ...), custom_call_target="tpu_custom_call" | custom-call | tf_op jit(solution)/shard_map/layer/pallas_call | solution.py:484
  99.9 0.6 copy.25
  100.5 0.6 copy.26
Async XLA Ops:
  0.6 0.7 copy-start.9
  0.6 0.7 copy-start.20
  0.7 0.7 copy-start.16
  0.7 0.7 copy-start.18
  0.7 0.7 copy-start.19
  0.7 0.7 copy-start.15
  0.7 0.7 copy-start.17
  1.4 1.2 %copy-start = (bf16[2,1024,256]{2,1,0:T(8,128)(2,1)S(1)}, bf16[2,1024,256]{2,1,0:T(8,128)(2,1)}, u32[]{:S(2)}) copy-start(bf16[2,1024,256]{2,1,0:T(8,128)(2,1)} %refs_12_.1) | copy-start | bytes 3145732
  2.6 1.2 %copy-start.1 = (bf16[2,1024,256]{2,1,0:T(8,128)(2,1)S(1)}, bf16[2,1024,256]{2,1,0:T(8,128)(2,1)}, u32[]{:S(2)}) copy-start(bf16[2,1024,256]{2,1,0:T(8,128)(2,1)} %refs_13_.1) | copy-start | bytes 3145732
  3.9 1.0 %copy-start.2 = (bf16[2048,128]{1,0:T(8,128)(2,1)S(1)}, bf16[2048,128]{1,0:T(8,128)(2,1)}, u32[]{:S(2)}) copy-start(bf16[2048,128]{1,0:T(8,128)(2,1)} %refs_15_.1) | copy-start | bytes 1572868
  4.9 1.0 %copy-start.3 = (bf16[2048,128]{1,0:T(8,128)(2,1)S(1)}, bf16[2048,128]{1,0:T(8,128)(2,1)}, u32[]{:S(2)}) copy-start(bf16[2048,128]{1,0:T(8,128)(2,1)} %refs_17_.1) | copy-start | bytes 1572868
  5.9 1.0 %copy-start.4 = (bf16[1,2048,128]{2,1,0:T(8,128)(2,1)S(1)}, bf16[1,2048,128]{2,1,0:T(8,128)(2,1)}, u32[]{:S(2)}) copy-start(bf16[1,2048,128]{2,1,0:T(8,128)(2,1)} %refs_18_.1) | copy-start | bytes 1572868
  7.0 1.0 %copy-start.5 = (bf16[1,2048,128]{2,1,0:T(8,128)(2,1)S(1)}, bf16[1,2048,128]{2,1,0:T(8,128)(2,1)}, u32[]{:S(2)}) copy-start(bf16[1,2048,128]{2,1,0:T(8,128)(2,1)} %refs_19_.1) | copy-start | bytes 1572868
  8.0 1.0 %copy-start.6 = (bf16[1,128,2048]{2,1,0:T(8,128)(2,1)S(1)}, bf16[1,128,2048]{2,1,0:T(8,128)(2,1)}, u32[]{:S(2)}) copy-start(bf16[1,128,2048]{2,1,0:T(8,128)(2,1)} %refs_20_.1) | copy-start | bytes 1572868
  9.1 0.9 copy-start.7
  10.0 0.7 copy-start.8
  10.7 0.7 copy-start.10
  11.4 0.7 copy-start.11
  12.1 0.7 copy-start.12
  12.8 0.7 copy-start.13
  13.5 0.7 copy-start.14
